TPU v7x, 32 devices: a whole 2x2x4 slice. The times are simulated.
32 devices in a mesh: grp: 2 (over y), ep: 8 (over z, x), tp: 2 (over core).
Axes of the slice: x: 2, y: 2, z: 4, core: 2. Of those that a mesh axis runs over, the one named last changes fastest.
Arguments:
- tokens: bfloat16 [256, 1024], P(('grp', 'ep')), parts along dimension 0, may hold values from -6 to 6
- query_weight: bfloat16 [1024, 512], P(None, 'tp'), may hold values from -0.1875 to 0.1875
- key_weight: bfloat16 [1024, 512], P(None, 'tp'), may hold values from -0.1875 to 0.1875
- value_weight: bfloat16 [1024, 512], P(None, 'tp'), may hold values from -0.1875 to 0.1875
- outgate_weight: bfloat16 [1024, 512], P(None, 'tp'), may hold values from -0.1875 to 0.1875
- ingate_weight: bfloat16 [1024, 4], P(None, 'tp'), may hold values from -0.1875 to 0.1875
- forget_weight: bfloat16 [1024, 4], P(None, 'tp'), may hold values from -0.1875 to 0.1875
- forget_bias: float32 [4], P('tp'), may hold values from -2 to 5
- head_gain: float32 [4, 128], P('tp'), may hold values from 0.1 to 1.9
- merge_weight: bfloat16 [512, 1024], P('tp'), may hold values from -0.25 to 0.25
- mixer_gain: float32 [1024], replicated, may hold values from 0.1 to 1.9
- feed_gain: float32 [1024], replicated, may hold values from 0.1 to 1.9
- memory_matrix: float32 [256, 4, 128, 128], P(('grp', 'ep'), 'tp'), parts along dimension 0, may hold values from -0.6 to 0.6
- memory_norm: float32 [256, 4, 128], P(('grp', 'ep'), 'tp'), parts along dimension 0, may hold values from -0.6 to 0.6
- memory_max: float32 [256, 4], P(('grp', 'ep'), 'tp'), parts along dimension 0, may hold values from -4 to 4
- routes: int32 [256, 2], P(('grp', 'ep')), parts along dimension 0, may hold values from 0 to 7, all different within a row; in each aligned block of 16 rows (0 to 15, 16 to 31, ...) at most 6 rows name the same one
- route_scores: bfloat16 [256, 2], P(('grp', 'ep')), parts along dimension 0, may hold values from -4 to 4
- expert_gate: bfloat16 [8, 1024, 1792], P('ep', None, 'tp'), may hold values from -0.1875 to 0.1875
- expert_up: bfloat16 [8, 1024, 1792], P('ep', None, 'tp'), may hold values from -0.1875 to 0.1875
- expert_down: bfloat16 [8, 1792, 1024], P('ep', 'tp'), may hold values from -0.125 to 0.125
- dense_left: bfloat16 [1024, 2816], P(None, 'ep'), may hold values from -0.1875 to 0.1875
- dense_right: bfloat16 [1024, 2816], P(None, 'ep'), may hold values from -0.1875 to 0.1875
- dense_down: bfloat16 [2816, 1024], P('ep'), may hold values from -0.109375 to 0.109375
- blend_weight: float32 [1024], replicated, may hold values from -0.1875 to 0.1875
Outputs:
- layer_out: bfloat16 [256, 1024], P(('grp', 'ep', 'tp')), parts along dimension 0
- new_matrix: float32 [256, 4, 128, 128], P(('grp', 'ep'), 'tp'), parts along dimension 0
- new_norm: float32 [256, 4, 128], P(('grp', 'ep'), 'tp'), parts along dimension 0
- new_max: float32 [256, 4], P(('grp', 'ep'), 'tp'), parts along dimension 0
There are 2 independent parts, one for each index of `grp`. A program takes and returns all parts, laid end to end along the dimension named above; an argument that names none is the same for every part. Nothing has to cross between parts.
Inputs may be any that keep to these rules, and one draw needn't show every extreme that they name: `routes`: each row names 2 different experts. Among the rows of one device (aligned blocks of 16 rows) no expert is named more than 6 times, and in every draw some expert is named exactly 6 times in some block.
All inputs are finite; a program needn't handle non-finite values.
Results may differ from a plain program's by a relative error of at most 0.014.
Values may be sent and summed in bfloat16 or wider, within the bound.
A program may use at most 64 MiB of HBM per device.

v0:
```python
import functools

import jax
import jax.numpy as jnp
from jax import lax
from jax.experimental import pallas as pl
from jax.experimental.pallas import tpu as pltpu
from jax.sharding import PartitionSpec as P

epsilon = 1e-06
F32 = jnp.float32
BF16 = jnp.bfloat16
MESH = pl.DeviceIdType.MESH
LANES = 128


def rms_rows(floats, gains):
    scaled = floats * lax.rsqrt(jnp.mean(floats * floats, axis=-1, keepdims=True) + epsilon)
    return (scaled * gains).astype(BF16)


def silu(x):
    return x / (1.0 + jnp.exp(-x))


def sigmoid(x):
    return 1.0 / (1.0 + jnp.exp(-x))


def eye_mask(n):
    return lax.broadcasted_iota(jnp.int32, (n, n), 0) == lax.broadcasted_iota(jnp.int32, (n, n), 1)


def to_column(row):
    return jnp.sum(jnp.where(eye_mask(row.shape[1]), row, 0.0), axis=1, keepdims=True)


def to_row(column):
    return jnp.sum(jnp.where(eye_mask(column.shape[0]), column, 0.0), axis=0, keepdims=True)


def dot_nt(a, b):
    return lax.dot_general(a, b, (((1,), (1,)), ((), ())), preferred_element_type=F32)


def flush_kernel(*refs):
    count = (len(refs) - 1) // 2
    copies = [
        pltpu.make_async_copy(refs[i], refs[count + i], refs[-1].at[i]) for i in range(count)
    ]
    for copy in copies:
        copy.start()
    for copy in copies:
        copy.wait()


def whole(ref, sem):
    return pltpu.make_async_copy(ref, ref, sem)


def flipped(me, k):
    peer, bit = me, 1
    while bit <= k:
        if k & bit:
            peer = peer + bit * (1 - 2 * ((me // bit) % 2))
        bit *= 2
    return peer


def feed_kernel(
    n_ep, n_tp, chunk, small, *refs,
):
    (
        tokens_hbm, wi_hbm, wf_hbm, bias_hbm, head_gain_hbm, mixer_gain_hbm, old_norm_hbm, old_max_hbm,
        feed_gain_hbm, blend_hbm, routes_hbm, scores_hbm,
    ) = refs[:small]
    (
        wq, wk, wv, wo, matrix_hbm, merge_hbm, gate_hbm, up_hbm, down_hbm, left_hbm, right_hbm, ddown_hbm,
        out, new_matrix, new_norm, new_max,
        wquery, wbuf, mbuf, spread, numer, aux, merge, gate_up, down, sides, ddown,
        head_send, head_recv, resid_buf, norm_buf, route_buf, route_all, route_far, every,
        hidden, part_send, part_recv, dense, ret_send, ret_recv,
        msem, wsem, head_sem, route_sem, ag_sem, ag_rsem, fwd_sem, part_sem, ret_sem,
    ) = refs[small : -small - 1]
    held, small_sems = refs[-small - 1 : -1], refs[-1]
    (
        tokens, wi, wf, bias, head_gain, mixer_gain, old_norm, old_max, feed_gain, blend_weight,
        routes, scores,
    ) = held

    small_copies = [
        pltpu.make_async_copy(refs[i], held[i], small_sems.at[i]) for i in range(small)
    ]
    wcopies = [
        pltpu.make_async_copy(ref, wbuf.at[i], wsem.at[0]) for i, ref in enumerate((wk, wv, wo))
    ]
    query_copy = pltpu.make_async_copy(wq, wquery, wsem.at[6])
    for copy in small_copies:
        copy.start()
    query_copy.start()

    me = lax.axis_index("ep")
    core = lax.axis_index("tp")
    partner = {"tp": 1 - core}
    rows, width = tokens.shape
    half = rows // n_tp
    hub = n_tp - 1
    side = n_ep // 2
    peers = {k: flipped(me, k) for k in range(1, n_ep)}
    far_ks, near_ks = list(range(n_ep - 1, side - 1, -1)), list(range(side - 1, 0, -1))
    near_first = (me // side) * side
    far_first = side - near_first

    barrier = pltpu.get_barrier_semaphore()
    pl.semaphore_signal(barrier, inc=1, device_id=partner, device_id_type=MESH)
    for k in far_ks + near_ks:
        pl.semaphore_signal(
            barrier, inc=1, device_id={"ep": peers[k], "tp": hub if k >= side else 0}, device_id_type=MESH
        )
    for copy in wcopies:
        copy.start()

    chunks = rows // chunk
    mcopies = [
        pltpu.make_async_copy(
            matrix_hbm.at[pl.ds(c * chunk, chunk)], mbuf.at[pl.ds(c * chunk, chunk)], msem.at[c]
        )
        for c in range(chunks)
    ]
    merge_copy = pltpu.make_async_copy(merge_hbm, merge, wsem.at[1])
    side_copies = [
        pltpu.make_async_copy(ref, sides.at[i], wsem.at[2]) for i, ref in enumerate((left_hbm, right_hbm))
    ]
    down_copy = pltpu.make_async_copy(down_hbm.at[0], down, wsem.at[3])
    ddown_copy = pltpu.make_async_copy(ddown_hbm, ddown, wsem.at[4])
    tiles = gate_up.shape[0]
    gu_copies = []
    for j in range(tiles):
        for column, ref in enumerate((gate_hbm, up_hbm)):
            gu_copies.append(
                pltpu.make_async_copy(
                    ref.at[0, :, pl.ds(j * LANES, LANES)],
                    gate_up.at[j, :, pl.ds(column * LANES, LANES)],
                    wsem.at[5],
                )
            )
    for copy in small_copies:
        copy.wait()
    for copy in mcopies + [merge_copy]:
        copy.start()

    heads, size = head_gain.shape
    inner = heads * size
    mixed = rms_rows(tokens[...].astype(F32), mixer_gain[...])
    mixed_f = mixed.astype(F32)
    keeps, writes, maxes = [], [], []
    for h in range(heads):
        in_gate = jnp.sum(mixed_f * wi[h : h + 1, :].astype(F32), axis=-1, keepdims=True)
        pre = jnp.sum(mixed_f * wf[h : h + 1, :].astype(F32), axis=-1, keepdims=True) + bias[:, h : h + 1]
        log_forget = jnp.minimum(pre, 0.0) - jnp.log1p(jnp.exp(-jnp.abs(pre)))
        old = to_column(old_max[h : h + 1, :])
        top = jnp.maximum(log_forget + old, in_gate)
        keeps.append(jnp.exp(log_forget + old - top))
        writes.append(jnp.exp(in_gate - top))
        maxes.append(top)

    query_copy.wait()
    query = jnp.dot(mixed, wquery[...], preferred_element_type=F32)
    high = query.astype(BF16)
    rest = query - high.astype(F32)
    middle = rest.astype(BF16)
    low = (rest - middle.astype(F32)).astype(BF16)
    terms = jnp.concatenate([high, middle, low], axis=0)
    lines = lax.broadcasted_iota(jnp.int32, (3 * rows, rows * size), 0)
    columns = lax.broadcasted_iota(jnp.int32, (3 * rows, rows * size), 1)
    pick = jnp.where(lax.rem(lines, rows) == columns // size, 1.0, 0.0).astype(BF16)
    spread[...] = lax.dot_general(
        terms, pick, (((0,), (0,)), ((), ())), preferred_element_type=F32
    )

    whole(wbuf, wsem.at[0]).wait()

    def project(i):
        return jnp.dot(mixed, wbuf[i], preferred_element_type=F32)

    keys = project(0) * size ** (-0.5)
    values = project(1)
    outgate = project(2)
    aux[:, :inner] = values
    denoms, crosses = [], []
    for h in range(heads):
        span = slice(h * size, (h + 1) * size)
        written = writes[h] * keys[:, span]
        aux[:, inner + h * size : inner + (h + 1) * size] = written
        fresh = keeps[h] * old_norm[:, h, :] + written
        new_norm[:, h, :] = fresh
        denoms.append(jnp.sum(query[:, span] * fresh, axis=-1, keepdims=True))
        crosses.append(jnp.sum(query[:, span] * written, axis=-1, keepdims=True))
    for c in range(chunks):
        mcopies[c].wait()
        for b in range(c * chunk, (c + 1) * chunk):
            for h in range(heads):
                numer[b : b + 1, h * size : (h + 1) * size] = jnp.sum(
                    spread[h * size : (h + 1) * size, b * size : (b + 1) * size] * mbuf[b, h],
                    axis=0,
                    keepdims=True,
                )
    energy = jnp.zeros((rows, 1), F32)
    gated = []
    for h in range(heads):
        span = slice(h * size, (h + 1) * size)
        readout = (keeps[h] * numer[:, span] + crosses[h] * values[:, span]) / jnp.maximum(
            jnp.abs(denoms[h]), jnp.exp(-maxes[h])
        )
        energy = energy + jnp.sum(readout * readout, axis=-1, keepdims=True)
        gated.append(
            (readout * head_gain[h : h + 1, :] * sigmoid(outgate[:, span])).astype(BF16)
        )
    merge_copy.wait()
    head_part = jnp.dot(
        jnp.concatenate(gated, axis=1), merge[...], preferred_element_type=F32
    )
    head_send[:, :width] = head_part
    head_send[:, width:] = jnp.broadcast_to(energy, (rows, LANES))

    @pl.when(core == hub)
    def _():
        pl.semaphore_wait(barrier, 2 * len(far_ks) + 1)

    @pl.when(core != hub)
    def _():
        pl.semaphore_wait(barrier, 2 * len(near_ks) + 1)

    head_copy = pltpu.make_async_remote_copy(
        head_send, head_recv, head_sem.at[0], head_sem.at[1], device_id=partner, device_id_type=MESH
    )
    head_copy.start()
    for copy in gu_copies + [down_copy]:
        copy.start()

    @pl.when(core == hub)
    def _():
        for copy in side_copies + [ddown_copy]:
            copy.start()

    def send(source, slot, send_sem, recv_sem, device):
        pltpu.make_async_remote_copy(
            source, slot, send_sem, recv_sem, device_id=device, device_id_type=MESH
        ).start()

    def all_others(slots, sem):
        return whole(slots.at[pl.ds(0, n_ep - 1)], sem)

    picks = routes.shape[0]
    score = scores[...].astype(F32)
    raised = jnp.exp(score - jnp.max(score, axis=0, keepdims=True))
    route_weight = raised / jnp.sum(raised, axis=0, keepdims=True)
    chosen = routes[...]
    route_buf[...] = jnp.zeros_like(route_buf)
    for e in range(n_ep):
        named = jnp.zeros((1, rows), F32)
        for p in range(picks):
            named = named + jnp.where(chosen[p : p + 1, :] == e, route_weight[p : p + 1, :], 0.0)
        route_buf[e, :, :rows] = named
    for h in range(heads):
        new_max[h : h + 1, :] = to_row(maxes[h])

    head_copy.wait()
    head_total = head_part + head_recv[:, :width]
    energy_total = energy + head_recv[:, width : width + 1]
    scale = lax.rsqrt(energy_total / (inner * n_tp) + epsilon)
    resid = (tokens[...].astype(F32) + scale * head_total).astype(BF16).astype(F32)
    norm_buf[...] = rms_rows(resid, feed_gain[...])

    def spread_rows(ks):
        for k in ks:
            send(norm_buf, every.at[me], ag_sem, ag_rsem.at[me], {"ep": peers[k], "tp": hub})
        for k in ks:
            send(
                route_buf.at[peers[k]], route_all.at[me], route_sem.at[0], route_sem.at[1],
                {"ep": peers[k], "tp": hub},
            )

    @pl.when(core == hub)
    def _():
        spread_rows(far_ks)

    @pl.when(core != hub)
    def _():
        spread_rows(near_ks)

    every[me] = norm_buf[...]
    route_all[me] = route_buf[me]

    for i in range(n_tp):
        resid_buf[i] = resid[i * half : (i + 1) * half]

    for h in range(heads):
        key_cols = aux[:, inner + h * size : inner + (h + 1) * size].T
        for b in range(rows):
            new_matrix[b, h] = (
                keeps[h][b : b + 1, :] * mbuf[b, h]
                + key_cols[:, b : b + 1] * aux[b : b + 1, h * size : (h + 1) * size]
            )

    @pl.when(core == hub)
    def _():
        for i in range(n_ep - 1):
            origin = i + (i - me + n_ep) // n_ep
            whole(every.at[origin], ag_rsem.at[origin]).wait()
            send(every.at[origin], every.at[origin], fwd_sem.at[0], fwd_sem.at[1], partner)

    @pl.when(core != hub)
    def _():
        all_others(every, fwd_sem.at[1]).wait()

    count = n_ep * rows
    whole(gate_up, wsem.at[5]).wait()
    all_rows = every[...].reshape(count, width)
    for j in range(tiles):
        both = jnp.dot(all_rows, gate_up[j], preferred_element_type=F32)
        hidden[:, j * LANES : (j + 1) * LANES] = (
            silu(both[:, :LANES]) * both[:, LANES:]
        ).astype(BF16)
    down_copy.wait()
    block = count // 2
    near_span = pl.ds(pl.multiple_of(near_first * rows, block), block)
    far_span = pl.ds(pl.multiple_of(far_first * rows, block), block)

    def part_of(span):
        return jnp.dot(hidden[span, :], down[...], preferred_element_type=F32).astype(BF16)

    def weights_of(table, first):
        weights = jnp.broadcast_to(table[pl.ds(first, side)], (side, rows, LANES)).reshape(block, LANES)
        token = lax.rem(lax.broadcasted_iota(jnp.int32, (block, LANES), 0), rows)
        lane = lax.broadcasted_iota(jnp.int32, (block, LANES), 1)
        return jnp.sum(jnp.where(lane == token, weights, 0.0), axis=-1, keepdims=True)

    def give_back(combined, ks, first):
        ret_send[...] = combined.reshape(side, n_tp, half, width).astype(BF16)
        for k in ks:
            for i in range(n_tp):
                send(
                    ret_send.at[peers[k] - first, i], ret_recv.at[me], ret_sem.at[0], ret_sem.at[1],
                    {"ep": peers[k], "tp": i},
                )

    @pl.when(core != hub)
    def _():
        part_send[...] = part_of(far_span)
        send(part_send, part_recv, part_sem.at[0], part_sem.at[1], partner)
        part = part_of(near_span).astype(F32)
        whole(route_far, route_sem.at[3]).wait()
        own_weight = weights_of(route_far, near_first)
        whole(part_recv, part_sem.at[1]).wait()
        give_back(own_weight * part + part_recv[...].astype(F32), near_ks, near_first)
        send(ret_send.at[me - near_first, hub], ret_recv.at[me], ret_sem.at[0], ret_sem.at[1], partner)
        ret_recv[me] = ret_send[me - near_first, 0]
        if near_ks:
            whole(route_all.at[pl.ds(0, side - 1)], route_sem.at[0]).wait()
            whole(every.at[pl.ds(0, side - 1)], ag_sem).wait()
        whole(part_send, part_sem.at[0]).wait()
        all_others(ret_recv, ret_sem.at[1]).wait()

    @pl.when(core == hub)
    def _():
        all_others(route_all, route_sem.at[1]).wait()
        send(route_all, route_far, route_sem.at[2], route_sem.at[3], partner)
        near_part = part_of(near_span).astype(F32)
        whole(sides, wsem.at[2]).wait()
        ddown_copy.wait()
        inputs = every[...].reshape(count, width)
        blend = sigmoid(jnp.sum(inputs.astype(F32) * blend_weight[...], axis=-1, keepdims=True))
        dense_hidden = (silu(dot_nt(inputs, sides[0])) * dot_nt(inputs, sides[1])).astype(BF16)
        dense[...] = blend * jnp.dot(dense_hidden, ddown[...], preferred_element_type=F32)
        part_send[...] = (weights_of(route_all, near_first) * near_part + dense[near_span, :]).astype(BF16)
        send(part_send, part_recv, part_sem.at[0], part_sem.at[1], partner)
        part = part_of(far_span).astype(F32)
        own_weight = weights_of(route_all, far_first)
        whole(part_recv, part_sem.at[1]).wait()
        expert_out = (part + part_recv[...].astype(F32)).astype(BF16).astype(F32)
        give_back(own_weight * expert_out + dense[far_span, :], far_ks, far_first)
        whole(route_all.at[pl.ds(0, side)], route_sem.at[0]).wait()
        whole(route_all, route_sem.at[2]).wait()
        whole(every.at[pl.ds(0, side)], ag_sem).wait()
        all_others(every, fwd_sem.at[0]).wait()
        whole(part_send, part_sem.at[0]).wait()
        whole(ret_recv, ret_sem.at[1]).wait()

    total = resid_buf[core]
    for e in range(n_ep):
        total = total + ret_recv[e].astype(F32)
    out[...] = total.astype(BF16)

    @pl.when(core == hub)
    def _():
        whole(ret_recv, ret_sem.at[0]).wait()

    @pl.when(core != hub)
    def _():
        all_others(ret_recv, ret_sem.at[0]).wait()


VMEM = pl.BlockSpec(memory_space=pltpu.VMEM)
ANY = pl.BlockSpec(memory_space=pl.ANY)


def local(
    n_ep, n_tp, tokens, query_weight, key_weight, value_weight, outgate_weight, ingate_weight,
    forget_weight, forget_bias, head_gain, merge_weight, mixer_gain, feed_gain, memory_matrix,
    memory_norm, memory_max, routes, route_scores, expert_gate, expert_up, expert_down,
    dense_left, dense_right, dense_down, blend_weight,
):
    rows, width = tokens.shape
    heads, size = head_gain.shape
    half = rows // n_tp
    chunk = max(1, rows // 2)
    chunks = rows // chunk
    dma = pltpu.SemaphoreType.DMA
    inner = expert_gate.shape[2]
    tiles = inner // LANES
    dense_inner = dense_left.shape[1]
    count = n_ep * rows
    lanes = heads * size
    small = (
        tokens, ingate_weight.T, forget_weight.T, forget_bias.reshape(1, heads), head_gain,
        mixer_gain.reshape(1, width), memory_norm, memory_max.T, feed_gain.reshape(1, width),
        blend_weight.reshape(1, width), routes.T, route_scores.T,
    )
    operands = (
        *small, query_weight, key_weight, value_weight, outgate_weight, memory_matrix, merge_weight, expert_gate, expert_up,
        expert_down, dense_left.T, dense_right.T, dense_down,
    )
    layer_half, matrix, norm_vec, new_max = pl.pallas_call(
        functools.partial(feed_kernel, n_ep, n_tp, chunk, len(small)),
        out_shape=(
            pltpu.VMEM((half, width), BF16),
            pltpu.VMEM(memory_matrix.shape, F32),
            pltpu.VMEM(memory_norm.shape, F32),
            pltpu.VMEM((heads, rows), F32),
        ),
        in_specs=[ANY] * (len(small) + 12),
        out_specs=(VMEM,) * 4,
        scratch_shapes=[
            pltpu.VMEM((width, lanes), BF16),
            pltpu.VMEM((3, width, lanes), BF16),
            pltpu.VMEM(memory_matrix.shape, F32),
            pltpu.VMEM((lanes, rows * size), F32),
            pltpu.VMEM((rows, lanes), F32),
            pltpu.VMEM((rows, 2 * lanes), F32),
            pltpu.VMEM(merge_weight.shape, BF16),
            pltpu.VMEM((tiles, width, 2 * LANES), BF16),
            pltpu.VMEM((inner, width), BF16),
            pltpu.VMEM((2, dense_inner, width), BF16),
            pltpu.VMEM((dense_inner, width), BF16),
            pltpu.VMEM((rows, width + LANES), F32),
            pltpu.VMEM((rows, width + LANES), F32),
            pltpu.VMEM((n_tp, half, width), F32),
            pltpu.VMEM((rows, width), BF16),
            pltpu.VMEM((n_ep, 1, LANES), F32),
            pltpu.VMEM((n_ep, 1, LANES), F32),
            pltpu.VMEM((n_ep, 1, LANES), F32),
            pltpu.VMEM((n_ep, rows, width), BF16),
            pltpu.VMEM((count, inner), BF16),
            pltpu.VMEM((count // 2, width), BF16),
            pltpu.VMEM((count // 2, width), BF16),
            pltpu.VMEM((count, width), F32),
            pltpu.VMEM((n_ep // 2, n_tp, half, width), BF16),
            pltpu.VMEM((n_ep, half, width), BF16),
            dma((chunks,)),
            dma((7,)),
            dma((2,)),
            dma((4,)),
            dma,
            dma((n_ep,)),
            dma((2,)),
            dma((2,)),
            dma((2,)),
            *(pltpu.VMEM(a.shape, a.dtype) for a in small),
            dma((len(small),)),
        ],
        compiler_params=pltpu.CompilerParams(
            collective_id=0, has_side_effects=True, vmem_limit_bytes=48 << 20
        ),
        name="feed_forward",
    )(*(pltpu.with_memory_space_constraint(a, pltpu.HBM) for a in operands))
    held = (layer_half, matrix, norm_vec, new_max)
    layer_out, matrix, norm_vec, new_max = pl.pallas_call(
        flush_kernel,
        out_shape=tuple(jax.ShapeDtypeStruct(a.shape, a.dtype) for a in held),
        in_specs=[VMEM] * 4,
        out_specs=(ANY,) * 4,
        scratch_shapes=[dma((4,))],
        compiler_params=pltpu.CompilerParams(vmem_limit_bytes=8 << 20),
        name="write_out",
    )(*held)
    return (layer_out, matrix, norm_vec, new_max.T)


def solution(mesh):
    row = ("grp", "ep")
    in_specs = (
        P(row, None),
        P(None, "tp"),
        P(None, "tp"),
        P(None, "tp"),
        P(None, "tp"),
        P(None, "tp"),
        P(None, "tp"),
        P("tp"),
        P("tp", None),
        P("tp", None),
        P(),
        P(),
        P(row, "tp", None, None),
        P(row, "tp", None),
        P(row, "tp"),
        P(row, None),
        P(row, None),
        P("ep", None, "tp"),
        P("ep", None, "tp"),
        P("ep", "tp", None),
        P(None, "ep"),
        P(None, "ep"),
        P("ep", None),
        P(),
    )
    out_specs = (
        P(("grp", "ep", "tp"), None),
        P(row, "tp", None, None),
        P(row, "tp", None),
        P(row, "tp"),
    )
    body = functools.partial(local, mesh.shape["ep"], mesh.shape["tp"])
    return jax.shard_map(body, mesh=mesh, in_specs=in_specs, out_specs=out_specs, check_vma=False)
```

profile of v0, /device:TPU:0, one launch (start us, length us, event | category | flops | bytes accessed | tf_op | source)
XLA Modules:
  0.0 22.2 jit_solution(244668673395658555)
XLA Ops:
  0.6 20.2 %feed_forward.1 = (bf16[8,1024]{1,0:T(8,128)(2,1)S(1)}, f32[16,2,128,128]{3,2,1,0:T(8,128)S(1)}, f32[16,2,128]{2,1,0:T(2,128)S(1)}, f32[2,16]{1,0:T(2,128)S(1)}) custom-call(bf16[16,1024]{1,0:T(8,128)(2,1)} %refs_0_.1, bf16[2,1024]{1,0:T(2,128)(2,1)} %bitcast.14, bf16[2,1024]{1,0:T(2,128)(2,1)} %bitcast.15, f32[1,2]{1,0:T(1,128)} %bitcast.21, ...), custom_call_target="tpu_custom_call" | custom-call | tf_op jit(solution)/shard_map/feed_forward/pallas_call | solution.py:434
  20.9 1.4 %write_out.1 = (bf16[8,1024]{1,0:T(8,128)(2,1)}, f32[16,2,128,128]{3,2,1,0:T(8,128)}, f32[16,2,128]{2,1,0:T(2,128)}, f32[2,16]{1,0:T(2,128)}) custom-call(bf16[8,1024]{1,0:T(8,128)(2,1)S(1)} %get-tuple-element.12.refs_0_, f32[16,2,128,128]{3,2,1,0:T(8,128)S(1)} %get-tuple-element.13.refs_1_, f32[16,2,128]{2,1,0:T(2,128)S(1)} %get-tuple-element.14.refs_2_, ...), custom_call_target="tpu_custom_call" | custom-call | tf_op jit(solution)/shard_map/write_out/pallas_call | solution.py:488
where the time goes:
time: 22.4 us; the launch traced here: 22.2 us
  Pallas kernels  21.6 us (96%)
  between operations  0.65 us (3%)
    pallas_call x1, Pallas kernels, local(): pl.pallas_call(functools.partial(feed_kernel, n_ep, n_tp, chunk, len(smal...  20.2 us
    pallas_call x1, Pallas kernels, local(): pl.pallas_call(flush_kernel, out_shape=tuple((jax.ShapeDtypeStruct(a.shap...  1.37 us

commit v1 on v0

--- a/solution.py
+++ b/solution.py
@@ -262,6 +262,23 @@
         for p in range(picks):
             named = named + jnp.where(chosen[p : p + 1, :] == e, route_weight[p : p + 1, :], 0.0)
         route_buf[e, :, :rows] = named
+    route_all[me] = route_buf[me]
+
+    def spread_routes(ks):
+        for k in ks:
+            send(
+                route_buf.at[peers[k]], route_all.at[me], route_sem.at[0], route_sem.at[1],
+                {"ep": peers[k], "tp": hub},
+            )
+
+    @pl.when(core == hub)
+    def _():
+        spread_routes(far_ks)
+
+    @pl.when(core != hub)
+    def _():
+        spread_routes(near_ks)
+
     for h in range(heads):
         new_max[h : h + 1, :] = to_row(maxes[h])
 
@@ -275,11 +292,6 @@
     def spread_rows(ks):
         for k in ks:
             send(norm_buf, every.at[me], ag_sem, ag_rsem.at[me], {"ep": peers[k], "tp": hub})
-        for k in ks:
-            send(
-                route_buf.at[peers[k]], route_all.at[me], route_sem.at[0], route_sem.at[1],
-                {"ep": peers[k], "tp": hub},
-            )
 
     @pl.when(core == hub)
     def _():
@@ -290,7 +302,6 @@
         spread_rows(near_ks)
 
     every[me] = norm_buf[...]
-    route_all[me] = route_buf[me]
 
     for i in range(n_tp):
         resid_buf[i] = resid[i * half : (i + 1) * half]
@@ -312,20 +323,22 @@
 
     @pl.when(core != hub)
     def _():
+        down_copy.wait()
+        whole(gate_up, wsem.at[5]).wait()
         all_others(every, fwd_sem.at[1]).wait()
 
     count = n_ep * rows
-    whole(gate_up, wsem.at[5]).wait()
-    all_rows = every[...].reshape(count, width)
-    for j in range(tiles):
-        both = jnp.dot(all_rows, gate_up[j], preferred_element_type=F32)
-        hidden[:, j * LANES : (j + 1) * LANES] = (
-            silu(both[:, :LANES]) * both[:, LANES:]
-        ).astype(BF16)
-    down_copy.wait()
     block = count // 2
     near_span = pl.ds(pl.multiple_of(near_first * rows, block), block)
     far_span = pl.ds(pl.multiple_of(far_first * rows, block), block)
+
+    def fill_hidden():
+        all_rows = every[...].reshape(count, width)
+        for j in range(tiles):
+            both = jnp.dot(all_rows, gate_up[j], preferred_element_type=F32)
+            hidden[:, j * LANES : (j + 1) * LANES] = (
+                silu(both[:, :LANES]) * both[:, LANES:]
+            ).astype(BF16)
 
     def part_of(span):
         return jnp.dot(hidden[span, :], down[...], preferred_element_type=F32).astype(BF16)
@@ -336,26 +349,36 @@
         lane = lax.broadcasted_iota(jnp.int32, (block, LANES), 1)
         return jnp.sum(jnp.where(lane == token, weights, 0.0), axis=-1, keepdims=True)
 
-    def give_back(combined, ks, first):
-        ret_send[...] = combined.reshape(side, n_tp, half, width).astype(BF16)
+    piece = width // 2
+    pieces = [slice(i * piece, (i + 1) * piece) for i in range(2)]
+
+    def give_back(i, combined, ks, first):
+        ret_send[i] = combined.reshape(side, n_tp, half, piece).astype(BF16)
         for k in ks:
-            for i in range(n_tp):
+            for c in range(n_tp):
                 send(
-                    ret_send.at[peers[k] - first, i], ret_recv.at[me], ret_sem.at[0], ret_sem.at[1],
-                    {"ep": peers[k], "tp": i},
+                    ret_send.at[i, peers[k] - first, c], ret_recv.at[me, i], ret_sem.at[0], ret_sem.at[1],
+                    {"ep": peers[k], "tp": c},
                 )
 
     @pl.when(core != hub)
     def _():
-        part_send[...] = part_of(far_span)
-        send(part_send, part_recv, part_sem.at[0], part_sem.at[1], partner)
+        fill_hidden()
+        for i in range(2):
+            part_send[i] = jnp.dot(
+                hidden[far_span, :], down[:, pieces[i]], preferred_element_type=F32
+            ).astype(BF16)
+            send(part_send.at[i], part_recv.at[i], part_sem.at[0], part_sem.at[1 + i], partner)
         part = part_of(near_span).astype(F32)
         whole(route_far, route_sem.at[3]).wait()
         own_weight = weights_of(route_far, near_first)
-        whole(part_recv, part_sem.at[1]).wait()
-        give_back(own_weight * part + part_recv[...].astype(F32), near_ks, near_first)
-        send(ret_send.at[me - near_first, hub], ret_recv.at[me], ret_sem.at[0], ret_sem.at[1], partner)
-        ret_recv[me] = ret_send[me - near_first, 0]
+        for i in range(2):
+            whole(part_recv.at[i], part_sem.at[1 + i]).wait()
+            give_back(i, own_weight * part[:, pieces[i]] + part_recv[i].astype(F32), near_ks, near_first)
+            send(
+                ret_send.at[i, me - near_first, hub], ret_recv.at[me, i], ret_sem.at[0], ret_sem.at[1], partner
+            )
+            ret_recv[me, i] = ret_send[i, me - near_first, 0]
         if near_ks:
             whole(route_all.at[pl.ds(0, side - 1)], route_sem.at[0]).wait()
             whole(every.at[pl.ds(0, side - 1)], ag_sem).wait()
@@ -364,22 +387,28 @@
 
     @pl.when(core == hub)
     def _():
+        down_copy.wait()
+        whole(gate_up, wsem.at[5]).wait()
+        whole(sides, wsem.at[2]).wait()
+        ddown_copy.wait()
         all_others(route_all, route_sem.at[1]).wait()
         send(route_all, route_far, route_sem.at[2], route_sem.at[3], partner)
+        fill_hidden()
         near_part = part_of(near_span).astype(F32)
-        whole(sides, wsem.at[2]).wait()
-        ddown_copy.wait()
+        part = part_of(far_span).astype(F32)
         inputs = every[...].reshape(count, width)
         blend = sigmoid(jnp.sum(inputs.astype(F32) * blend_weight[...], axis=-1, keepdims=True))
         dense_hidden = (silu(dot_nt(inputs, sides[0])) * dot_nt(inputs, sides[1])).astype(BF16)
         dense[...] = blend * jnp.dot(dense_hidden, ddown[...], preferred_element_type=F32)
-        part_send[...] = (weights_of(route_all, near_first) * near_part + dense[near_span, :]).astype(BF16)
-        send(part_send, part_recv, part_sem.at[0], part_sem.at[1], partner)
-        part = part_of(far_span).astype(F32)
+        near_sum = (weights_of(route_all, near_first) * near_part + dense[near_span, :]).astype(BF16)
+        for i in range(2):
+            part_send[i] = near_sum[:, pieces[i]]
+            send(part_send.at[i], part_recv.at[i], part_sem.at[0], part_sem.at[1 + i], partner)
         own_weight = weights_of(route_all, far_first)
-        whole(part_recv, part_sem.at[1]).wait()
-        expert_out = (part + part_recv[...].astype(F32)).astype(BF16).astype(F32)
-        give_back(own_weight * expert_out + dense[far_span, :], far_ks, far_first)
+        for i in range(2):
+            whole(part_recv.at[i], part_sem.at[1 + i]).wait()
+            expert_out = (part[:, pieces[i]] + part_recv[i].astype(F32)).astype(BF16).astype(F32)
+            give_back(i, own_weight * expert_out + dense[far_span, pieces[i]], far_ks, far_first)
         whole(route_all.at[pl.ds(0, side)], route_sem.at[0]).wait()
         whole(route_all, route_sem.at[2]).wait()
         whole(every.at[pl.ds(0, side)], ag_sem).wait()
@@ -387,10 +416,11 @@
         whole(part_send, part_sem.at[0]).wait()
         whole(ret_recv, ret_sem.at[1]).wait()
 
-    total = resid_buf[core]
-    for e in range(n_ep):
-        total = total + ret_recv[e].astype(F32)
-    out[...] = total.astype(BF16)
+    for i in range(2):
+        total = resid_buf[core, :, pieces[i]]
+        for e in range(n_ep):
+            total = total + ret_recv[e, i].astype(F32)
+        out[:, pieces[i]] = total.astype(BF16)
 
     @pl.when(core == hub)
     def _():
@@ -462,11 +492,11 @@
             pltpu.VMEM((n_ep, 1, LANES), F32),
             pltpu.VMEM((n_ep, rows, width), BF16),
             pltpu.VMEM((count, inner), BF16),
-            pltpu.VMEM((count // 2, width), BF16),
-            pltpu.VMEM((count // 2, width), BF16),
+            pltpu.VMEM((2, count // 2, width // 2), BF16),
+            pltpu.VMEM((2, count // 2, width // 2), BF16),
             pltpu.VMEM((count, width), F32),
-            pltpu.VMEM((n_ep // 2, n_tp, half, width), BF16),
-            pltpu.VMEM((n_ep, half, width), BF16),
+            pltpu.VMEM((2, n_ep // 2, n_tp, half, width // 2), BF16),
+            pltpu.VMEM((n_ep, 2, half, width // 2), BF16),
             dma((chunks,)),
             dma((7,)),
             dma((2,)),
@@ -474,7 +504,7 @@
             dma,
             dma((n_ep,)),
             dma((2,)),
-            dma((2,)),
+            dma((3,)),
             dma((2,)),
             *(pltpu.VMEM(a.shape, a.dtype) for a in small),
             dma((len(small),)),

time: 22.4 us -> 22.2 us (level)
  no operation moved by 1% of the time
where the time goes in v1:
time: 22.2 us; the launch traced here: 22.1 us
  Pallas kernels  21.4 us (96%)
  between operations  0.65 us (3%)
    pallas_call x1, Pallas kernels, local(): pl.pallas_call(functools.partial(feed_kernel, n_ep, n_tp, chunk, len(smal...  20.1 us
    pallas_call x1, Pallas kernels, local(): pl.pallas_call(flush_kernel, out_shape=tuple((jax.ShapeDtypeStruct(a.shap...  1.37 us

profile of v1, /device:TPU:0, one launch (start us, length us, event | category | flops | bytes accessed | tf_op | source)
XLA Modules:
  0.0 22.1 jit_solution(7658477388624872939)
XLA Ops:
  0.6 20.1 %feed_forward.1 = (bf16[8,1024]{1,0:T(8,128)(2,1)S(1)}, f32[16,2,128,128]{3,2,1,0:T(8,128)S(1)}, f32[16,2,128]{2,1,0:T(2,128)S(1)}, f32[2,16]{1,0:T(2,128)S(1)}) custom-call(bf16[16,1024]{1,0:T(8,128)(2,1)} %refs_0_.1, bf16[2,1024]{1,0:T(2,128)(2,1)} %bitcast.14, bf16[2,1024]{1,0:T(2,128)(2,1)} %bitcast.15, f32[1,2]{1,0:T(1,128)} %bitcast.21, ...), custom_call_target="tpu_custom_call" | custom-call | tf_op jit(solution)/shard_map/feed_forward/pallas_call | solution.py:464
  20.7 1.4 %write_out.1 = (bf16[8,1024]{1,0:T(8,128)(2,1)}, f32[16,2,128,128]{3,2,1,0:T(8,128)}, f32[16,2,128]{2,1,0:T(2,128)}, f32[2,16]{1,0:T(2,128)}) custom-call(bf16[8,1024]{1,0:T(8,128)(2,1)S(1)} %get-tuple-element.12.refs_0_, f32[16,2,128,128]{3,2,1,0:T(8,128)S(1)} %get-tuple-element.13.refs_1_, f32[16,2,128]{2,1,0:T(2,128)S(1)} %get-tuple-element.14.refs_2_, ...), custom_call_target="tpu_custom_call" | custom-call | tf_op jit(solution)/shard_map/write_out/pallas_call | solution.py:518

commit v2 on v0

--- a/solution.py
+++ b/solution.py
@@ -107,16 +107,21 @@
     hub = n_tp - 1
     side = n_ep // 2
     peers = {k: flipped(me, k) for k in range(1, n_ep)}
-    far_ks, near_ks = list(range(n_ep - 1, side - 1, -1)), list(range(side - 1, 0, -1))
+    upper = me // side
+    near_peers = [peers[k] for k in range(side - 1, 0, -1)]
+    far_peers = []
+    for j in range(side // 2):
+        pair = (1 - upper) * (side - 1 - j) + upper * j
+        far_peers += [2 * pair + 1 - me % 2, 2 * pair + me % 2]
     near_first = (me // side) * side
     far_first = side - near_first
 
     barrier = pltpu.get_barrier_semaphore()
     pl.semaphore_signal(barrier, inc=1, device_id=partner, device_id_type=MESH)
-    for k in far_ks + near_ks:
-        pl.semaphore_signal(
-            barrier, inc=1, device_id={"ep": peers[k], "tp": hub if k >= side else 0}, device_id_type=MESH
-        )
+    for peer in far_peers:
+        pl.semaphore_signal(barrier, inc=1, device_id={"ep": peer, "tp": hub}, device_id_type=MESH)
+    for peer in near_peers:
+        pl.semaphore_signal(barrier, inc=1, device_id={"ep": peer, "tp": 0}, device_id_type=MESH)
     for copy in wcopies:
         copy.start()
 
@@ -225,11 +230,11 @@
 
     @pl.when(core == hub)
     def _():
-        pl.semaphore_wait(barrier, 2 * len(far_ks) + 1)
+        pl.semaphore_wait(barrier, 2 * len(far_peers) + 1)
 
     @pl.when(core != hub)
     def _():
-        pl.semaphore_wait(barrier, 2 * len(near_ks) + 1)
+        pl.semaphore_wait(barrier, 2 * len(near_peers) + 1)
 
     head_copy = pltpu.make_async_remote_copy(
         head_send, head_recv, head_sem.at[0], head_sem.at[1], device_id=partner, device_id_type=MESH
@@ -262,6 +267,23 @@
         for p in range(picks):
             named = named + jnp.where(chosen[p : p + 1, :] == e, route_weight[p : p + 1, :], 0.0)
         route_buf[e, :, :rows] = named
+    route_all[me] = route_buf[me]
+
+    def spread_routes(targets):
+        for peer in targets:
+            send(
+                route_buf.at[peer], route_all.at[me], route_sem.at[0], route_sem.at[1],
+                {"ep": peer, "tp": hub},
+            )
+
+    @pl.when(core == hub)
+    def _():
+        spread_routes(far_peers)
+
+    @pl.when(core != hub)
+    def _():
+        spread_routes(near_peers)
+
     for h in range(heads):
         new_max[h : h + 1, :] = to_row(maxes[h])
 
@@ -272,25 +294,19 @@
     resid = (tokens[...].astype(F32) + scale * head_total).astype(BF16).astype(F32)
     norm_buf[...] = rms_rows(resid, feed_gain[...])
 
-    def spread_rows(ks):
-        for k in ks:
-            send(norm_buf, every.at[me], ag_sem, ag_rsem.at[me], {"ep": peers[k], "tp": hub})
-        for k in ks:
-            send(
-                route_buf.at[peers[k]], route_all.at[me], route_sem.at[0], route_sem.at[1],
-                {"ep": peers[k], "tp": hub},
-            )
-
-    @pl.when(core == hub)
-    def _():
-        spread_rows(far_ks)
+    def spread_rows(targets):
+        for peer in targets:
+            send(norm_buf, every.at[me], ag_sem, ag_rsem.at[me], {"ep": peer, "tp": hub})
+
+    @pl.when(core == hub)
+    def _():
+        spread_rows(far_peers)
 
     @pl.when(core != hub)
     def _():
-        spread_rows(near_ks)
+        spread_rows(near_peers)
 
     every[me] = norm_buf[...]
-    route_all[me] = route_buf[me]
 
     for i in range(n_tp):
         resid_buf[i] = resid[i * half : (i + 1) * half]
@@ -312,20 +328,22 @@
 
     @pl.when(core != hub)
     def _():
+        down_copy.wait()
+        whole(gate_up, wsem.at[5]).wait()
         all_others(every, fwd_sem.at[1]).wait()
 
     count = n_ep * rows
-    whole(gate_up, wsem.at[5]).wait()
-    all_rows = every[...].reshape(count, width)
-    for j in range(tiles):
-        both = jnp.dot(all_rows, gate_up[j], preferred_element_type=F32)
-        hidden[:, j * LANES : (j + 1) * LANES] = (
-            silu(both[:, :LANES]) * both[:, LANES:]
-        ).astype(BF16)
-    down_copy.wait()
     block = count // 2
     near_span = pl.ds(pl.multiple_of(near_first * rows, block), block)
     far_span = pl.ds(pl.multiple_of(far_first * rows, block), block)
+
+    def fill_hidden():
+        all_rows = every[...].reshape(count, width)
+        for j in range(tiles):
+            both = jnp.dot(all_rows, gate_up[j], preferred_element_type=F32)
+            hidden[:, j * LANES : (j + 1) * LANES] = (
+                silu(both[:, :LANES]) * both[:, LANES:]
+            ).astype(BF16)
 
     def part_of(span):
         return jnp.dot(hidden[span, :], down[...], preferred_element_type=F32).astype(BF16)
@@ -336,27 +354,28 @@
         lane = lax.broadcasted_iota(jnp.int32, (block, LANES), 1)
         return jnp.sum(jnp.where(lane == token, weights, 0.0), axis=-1, keepdims=True)
 
-    def give_back(combined, ks, first):
+    def give_back(combined, targets, first):
         ret_send[...] = combined.reshape(side, n_tp, half, width).astype(BF16)
-        for k in ks:
+        for peer in targets:
             for i in range(n_tp):
                 send(
-                    ret_send.at[peers[k] - first, i], ret_recv.at[me], ret_sem.at[0], ret_sem.at[1],
-                    {"ep": peers[k], "tp": i},
+                    ret_send.at[peer - first, i], ret_recv.at[me], ret_sem.at[0], ret_sem.at[1],
+                    {"ep": peer, "tp": i},
                 )
 
     @pl.when(core != hub)
     def _():
+        fill_hidden()
         part_send[...] = part_of(far_span)
         send(part_send, part_recv, part_sem.at[0], part_sem.at[1], partner)
         part = part_of(near_span).astype(F32)
         whole(route_far, route_sem.at[3]).wait()
         own_weight = weights_of(route_far, near_first)
         whole(part_recv, part_sem.at[1]).wait()
-        give_back(own_weight * part + part_recv[...].astype(F32), near_ks, near_first)
+        give_back(own_weight * part + part_recv[...].astype(F32), near_peers, near_first)
         send(ret_send.at[me - near_first, hub], ret_recv.at[me], ret_sem.at[0], ret_sem.at[1], partner)
         ret_recv[me] = ret_send[me - near_first, 0]
-        if near_ks:
+        if near_peers:
             whole(route_all.at[pl.ds(0, side - 1)], route_sem.at[0]).wait()
             whole(every.at[pl.ds(0, side - 1)], ag_sem).wait()
         whole(part_send, part_sem.at[0]).wait()
@@ -364,11 +383,14 @@
 
     @pl.when(core == hub)
     def _():
+        down_copy.wait()
+        whole(gate_up, wsem.at[5]).wait()
+        whole(sides, wsem.at[2]).wait()
+        ddown_copy.wait()
         all_others(route_all, route_sem.at[1]).wait()
         send(route_all, route_far, route_sem.at[2], route_sem.at[3], partner)
+        fill_hidden()
         near_part = part_of(near_span).astype(F32)
-        whole(sides, wsem.at[2]).wait()
-        ddown_copy.wait()
         inputs = every[...].reshape(count, width)
         blend = sigmoid(jnp.sum(inputs.astype(F32) * blend_weight[...], axis=-1, keepdims=True))
         dense_hidden = (silu(dot_nt(inputs, sides[0])) * dot_nt(inputs, sides[1])).astype(BF16)
@@ -379,7 +401,7 @@
         own_weight = weights_of(route_all, far_first)
         whole(part_recv, part_sem.at[1]).wait()
         expert_out = (part + part_recv[...].astype(F32)).astype(BF16).astype(F32)
-        give_back(own_weight * expert_out + dense[far_span, :], far_ks, far_first)
+        give_back(own_weight * expert_out + dense[far_span, :], far_peers, far_first)
         whole(route_all.at[pl.ds(0, side)], route_sem.at[0]).wait()
         whole(route_all, route_sem.at[2]).wait()
         whole(every.at[pl.ds(0, side)], ag_sem).wait()

time: 22.4 us -> 22 us (0.982)
  Pallas kernels: 21.6 us -> 21.2 us
    pallas_call x1, Pallas kernels: 20.2 us -> 19.8 us  [local(): pl.pallas_call(functools.partial(feed_kernel, n_ep, n_tp, chunk, len(smal...]
where the time goes in v2:
time: 22 us; the launch traced here: 21.8 us
  Pallas kernels  21.2 us (96%)
  between operations  0.65 us (3%)
    pallas_call x1, Pallas kernels, local(): pl.pallas_call(functools.partial(feed_kernel, n_ep, n_tp, chunk, len(smal...  19.8 us
    pallas_call x1, Pallas kernels, local(): pl.pallas_call(flush_kernel, out_shape=tuple((jax.ShapeDtypeStruct(a.shap...  1.37 us

profile of v2, /device:TPU:0, one launch (start us, length us, event | category | flops | bytes accessed | tf_op | source)
XLA Modules:
  0.0 21.8 jit_solution(3532431804273483473)
XLA Ops:
  0.6 19.8 %feed_forward.1 = (bf16[8,1024]{1,0:T(8,128)(2,1)S(1)}, f32[16,2,128,128]{3,2,1,0:T(8,128)S(1)}, f32[16,2,128]{2,1,0:T(2,128)S(1)}, f32[2,16]{1,0:T(2,128)S(1)}) custom-call(bf16[16,1024]{1,0:T(8,128)(2,1)} %refs_0_.1, bf16[2,1024]{1,0:T(2,128)(2,1)} %bitcast.14, bf16[2,1024]{1,0:T(2,128)(2,1)} %bitcast.15, f32[1,2]{1,0:T(1,128)} %bitcast.21, ...), custom_call_target="tpu_custom_call" | custom-call | tf_op jit(solution)/shard_map/feed_forward/pallas_call | solution.py:456
  20.5 1.4 %write_out.1 = (bf16[8,1024]{1,0:T(8,128)(2,1)}, f32[16,2,128,128]{3,2,1,0:T(8,128)}, f32[16,2,128]{2,1,0:T(2,128)}, f32[2,16]{1,0:T(2,128)}) custom-call(bf16[8,1024]{1,0:T(8,128)(2,1)S(1)} %get-tuple-element.12.refs_0_, f32[16,2,128,128]{3,2,1,0:T(8,128)S(1)} %get-tuple-element.13.refs_1_, f32[16,2,128]{2,1,0:T(2,128)S(1)} %get-tuple-element.14.refs_2_, ...), custom_call_target="tpu_custom_call" | custom-call | tf_op jit(solution)/shard_map/write_out/pallas_call | solution.py:510

commit v3 on v2

--- a/solution.py
+++ b/solution.py
@@ -391,13 +391,13 @@
         send(route_all, route_far, route_sem.at[2], route_sem.at[3], partner)
         fill_hidden()
         near_part = part_of(near_span).astype(F32)
+        part = part_of(far_span).astype(F32)
         inputs = every[...].reshape(count, width)
         blend = sigmoid(jnp.sum(inputs.astype(F32) * blend_weight[...], axis=-1, keepdims=True))
         dense_hidden = (silu(dot_nt(inputs, sides[0])) * dot_nt(inputs, sides[1])).astype(BF16)
         dense[...] = blend * jnp.dot(dense_hidden, ddown[...], preferred_element_type=F32)
         part_send[...] = (weights_of(route_all, near_first) * near_part + dense[near_span, :]).astype(BF16)
         send(part_send, part_recv, part_sem.at[0], part_sem.at[1], partner)
-        part = part_of(far_span).astype(F32)
         own_weight = weights_of(route_all, far_first)
         whole(part_recv, part_sem.at[1]).wait()
         expert_out = (part + part_recv[...].astype(F32)).astype(BF16).astype(F32)

time: 22 us -> 22 us (level)
  no operation moved by 1% of the time
where the time goes in v3:
time: 22 us; the launch traced here: 21.8 us
  Pallas kernels  21.2 us (96%)
  between operations  0.65 us (3%)
    pallas_call x1, Pallas kernels, local(): pl.pallas_call(functools.partial(feed_kernel, n_ep, n_tp, chunk, len(smal...  19.8 us
    pallas_call x1, Pallas kernels, local(): pl.pallas_call(flush_kernel, out_shape=tuple((jax.ShapeDtypeStruct(a.shap...  1.37 us

profile of v3, /device:TPU:0, one launch (start us, length us, event | category | flops | bytes accessed | tf_op | source)
XLA Modules:
  0.0 21.8 jit_solution(11162340375761142825)
XLA Ops:
  0.6 19.8 %feed_forward.1 = (bf16[8,1024]{1,0:T(8,128)(2,1)S(1)}, f32[16,2,128,128]{3,2,1,0:T(8,128)S(1)}, f32[16,2,128]{2,1,0:T(2,128)S(1)}, f32[2,16]{1,0:T(2,128)S(1)}) custom-call(bf16[16,1024]{1,0:T(8,128)(2,1)} %refs_0_.1, bf16[2,1024]{1,0:T(2,128)(2,1)} %bitcast.14, bf16[2,1024]{1,0:T(2,128)(2,1)} %bitcast.15, f32[1,2]{1,0:T(1,128)} %bitcast.21, ...), custom_call_target="tpu_custom_call" | custom-call | tf_op jit(solution)/shard_map/feed_forward/pallas_call | solution.py:456
  20.4 1.4 %write_out.1 = (bf16[8,1024]{1,0:T(8,128)(2,1)}, f32[16,2,128,128]{3,2,1,0:T(8,128)}, f32[16,2,128]{2,1,0:T(2,128)}, f32[2,16]{1,0:T(2,128)}) custom-call(bf16[8,1024]{1,0:T(8,128)(2,1)S(1)} %get-tuple-element.12.refs_0_, f32[16,2,128,128]{3,2,1,0:T(8,128)S(1)} %get-tuple-element.13.refs_1_, f32[16,2,128]{2,1,0:T(2,128)S(1)} %get-tuple-element.14.refs_2_, ...), custom_call_target="tpu_custom_call" | custom-call | tf_op jit(solution)/shard_map/write_out/pallas_call | solution.py:510
